TPU v7x, 32 devices: a whole 2x2x4 slice. The times are simulated.
32 devices in a mesh: ep: 8 (over z, x), tp: 4 (over y, core).
Axes of the slice: x: 2, y: 2, z: 4, core: 2. Of those that a mesh axis runs over, the one named last changes fastest.
Arguments:
- pool_input: bfloat16 [2048, 2048], P('ep', 'tp'), may hold values from -6 to 6
- pool_map: bfloat16 [16, 128, 128], replicated, may hold values from -0.5 to 0.5
- pool_scale: float32 [2048], replicated, may hold values from 0.1 to 1.9
- out_proj: bfloat16 [2048, 4096], P('tp'), may hold values from -0.125 to 0.125
- moe_input: bfloat16 [1024, 4096], P('ep'), may hold values from -6 to 6
- norm_gain: float32 [4096], replicated, may hold values from 0.1 to 1.9
- routes: int32 [1024, 4], P('ep'), may hold values from 0 to 7, all different within a row; in each aligned block of 128 rows (0 to 127, 128 to 255, ...) at most 96 rows name the same one
- route_weights: float32 [1024, 4], P('ep'), may hold values from 0.1 to 1
- expert_gate: bfloat16 [8, 4096, 1024], P('ep', None, 'tp'), may hold values from -0.09375 to 0.09375
- expert_up: bfloat16 [8, 4096, 1024], P('ep', None, 'tp'), may hold values from -0.09375 to 0.09375
- expert_down: bfloat16 [8, 1024, 4096], P('ep', None, 'tp'), may hold values from -0.1875 to 0.1875
- shared_gate: bfloat16 [4096, 512], P(None, 'tp'), may hold values from -0.09375 to 0.09375
- shared_up: bfloat16 [4096, 512], P(None, 'tp'), may hold values from -0.09375 to 0.09375
- shared_down: bfloat16 [512, 4096], P('tp'), may hold values from -0.25 to 0.25
Outputs:
- mixer_output: bfloat16 [2048, 4096], P('ep', 'tp')
- moe_output: bfloat16 [1024, 4096], P('ep', 'tp')
Inputs may be any that keep to these rules, and one draw needn't show every extreme that they name: `routes`: each row names 4 different experts. In each aligned block of 128 rows no expert is named by more than 96 rows, a bound that some block reaches.
All inputs are finite; a program needn't handle non-finite values.
Results may differ from a plain program's by a relative error of at most 0.017.
Values may be sent and summed in bfloat16 or wider, within the bound.
A program may use at most 64 MiB of HBM per device.

v0:
```python
import jax
import jax.numpy as jnp
from jax import lax
from jax.experimental import pallas as pl
from jax.experimental.pallas import tpu as pltpu
from jax.sharding import PartitionSpec as P

windows = (2, 4, 8, 16)
reach_back = 15
eps = 1e-05


def passed_along(block, axis, distance):
    devices = range(lax.axis_size(axis))
    route = [(i - distance, i) for i in devices if i - distance in devices]
    return lax.ppermute(block, axis, route)


def pool_branch(pool_input, pool_map, pool_scale, out_proj):
    row_count = pool_input.shape[0]
    channels = pool_input.shape[1]
    group_dim = pool_map.shape[1]
    local_groups = channels // group_dim
    tp_rank = lax.axis_index("tp")
    ep_rank = lax.axis_index("ep")
    earlier_rows = passed_along(pool_input[row_count - reach_back :], "ep", 1)
    values = pool_input.astype(jnp.float32)
    extended = jnp.concatenate([earlier_rows.astype(jnp.float32), values], axis=0)
    position = (ep_rank * row_count + jnp.arange(row_count, dtype=jnp.int32)).astype(jnp.float32)
    group_ids = tp_rank * local_groups + jnp.arange(channels, dtype=jnp.int32) // group_dim
    group_kind = group_ids % 4
    running = jnp.zeros((row_count, channels), jnp.float32)
    pooled = -values
    for lag_step in range(reach_back + 1):
        running = running + extended[reach_back - lag_step : reach_back - lag_step + row_count]
        if lag_step + 1 in windows:
            kind_id = windows.index(lag_step + 1)
            counts = jnp.minimum(position + 1.0, float(lag_step + 1))
            select = (group_kind == kind_id).astype(jnp.float32)
            pooled = pooled + select[None, :] * running / counts[:, None]
    pooled = pooled.astype(jnp.bfloat16)
    my_maps = lax.dynamic_slice_in_dim(pool_map, tp_rank * local_groups, local_groups, 0)
    my_scale = lax.dynamic_slice_in_dim(pool_scale, tp_rank * channels, channels, 0)
    mapped = jnp.einsum(
        "rgc,gcd->rgd",
        pooled.reshape(row_count, local_groups, group_dim),
        my_maps,
        preferred_element_type=jnp.float32,
    )
    group_out = (mapped.reshape(row_count, channels) * my_scale[None, :]).astype(jnp.bfloat16)
    return jnp.dot(group_out, out_proj, preferred_element_type=jnp.float32)


def dispatch_rows(routes, expert_count, capacity):
    tok_count, top_count = routes.shape
    flat_ids = routes.reshape(tok_count * top_count)
    one_hot = (flat_ids[:, None] == jnp.arange(expert_count, dtype=jnp.int32)[None, :]).astype(
        jnp.int32
    )
    earlier = jnp.cumsum(one_hot, axis=0) - one_hot
    slot_ids = jnp.sum(earlier * one_hot, axis=1)
    return (flat_ids * capacity + slot_ids).reshape(tok_count, top_count)


def per_device(
    pool_input,
    pool_map,
    pool_scale,
    out_proj,
    moe_input,
    norm_gain,
    routes,
    route_weights,
    expert_gate,
    expert_up,
    expert_down,
    shared_gate,
    shared_up,
    shared_down,
):
    mixer_part = pool_branch(pool_input, pool_map, pool_scale, out_proj)
    values = moe_input.astype(jnp.float32)
    centre = values - jnp.mean(values, axis=1, keepdims=True)
    variance = jnp.mean(centre * centre, axis=1, keepdims=True)
    normed = (centre * lax.rsqrt(variance + eps) * norm_gain[None, :]).astype(jnp.bfloat16)
    expert_count = lax.axis_size("ep")
    tok_count = moe_input.shape[0]
    top_count = routes.shape[1]
    capacity = (3 * tok_count * top_count + 2 * expert_count - 1) // (2 * expert_count)
    slot_index = dispatch_rows(routes, expert_count, capacity)
    buffer_len = expert_count * capacity
    targets = jnp.arange(buffer_len, dtype=jnp.int32)[:, None]
    placing = jnp.zeros((buffer_len, tok_count), jnp.float32)
    for top_step in range(top_count):
        placing = placing + (targets == slot_index[None, :, top_step]).astype(jnp.float32)
    outgoing = jnp.dot(
        placing.astype(jnp.bfloat16), normed, preferred_element_type=jnp.float32
    ).astype(jnp.bfloat16)
    gate_weight = expert_gate[0]
    up_weight = expert_up[0]
    down_weight = expert_down[0]
    tp_rank = lax.axis_index("tp")
    slice_width = outgoing.shape[1] // lax.axis_size("tp")
    my_slice = lax.dynamic_slice_in_dim(outgoing, tp_rank * slice_width, slice_width, 1)
    arrived = lax.all_to_all(my_slice, "ep", split_axis=0, concat_axis=0, tiled=True)
    shard_cols = lax.all_gather(arrived, "tp", axis=1, tiled=True)
    gate_val = jnp.dot(shard_cols, gate_weight, preferred_element_type=jnp.float32)
    up_val = jnp.dot(shard_cols, up_weight, preferred_element_type=jnp.float32)
    hidden = (jax.nn.silu(gate_val) * up_val).astype(jnp.bfloat16)
    expert_result = jnp.dot(
        lax.all_gather(hidden, "tp", axis=1, tiled=True),
        down_weight,
        preferred_element_type=jnp.float32,
    ).astype(jnp.bfloat16)
    returned = lax.all_to_all(expert_result, "ep", split_axis=0, concat_axis=0, tiled=True)
    routed = jnp.zeros((tok_count, returned.shape[1]), jnp.float32)
    for top_step in range(top_count):
        picked = returned[slot_index[:, top_step]].astype(jnp.float32)
        routed = routed + route_weights[:, top_step, None] * picked
    shared_gate_val = jnp.dot(normed, shared_gate, preferred_element_type=jnp.float32)
    shared_up_val = jnp.dot(normed, shared_up, preferred_element_type=jnp.float32)
    shared_hidden = (jax.nn.silu(shared_gate_val) * shared_up_val).astype(jnp.bfloat16)
    shared_part = jnp.dot(shared_hidden, shared_down, preferred_element_type=jnp.float32)
    mixer_sum, shared_sum = (
        lax.psum_scatter(
            mixer_part.astype(jnp.bfloat16), "tp", scatter_dimension=1, tiled=True
        ).astype(jnp.float32),
        lax.psum_scatter(
            shared_part.astype(jnp.bfloat16), "tp", scatter_dimension=1, tiled=True
        ).astype(jnp.float32),
    )
    return (mixer_sum.astype(jnp.bfloat16), (routed + shared_sum).astype(jnp.bfloat16))


HALO = 16
Z_SIDE, X_SIDE, Y_SIDE, CORES = 4, 2, 2, 2


def fused_kernel(
    pool_h, map_h, scale_h, proj_h, moe_h, gain_h, wt_h, gate_h, up_h, down_h, sg_h, su_h, sd_h,
    mix_out, moe_out,
    pool_v, map_v, scale_v, proj_v, moe_v, gain_v, gate_v, up_v, down_v, sg_v, su_v, sd_v,
    halo_v, ext_v, group_v, mix_v, mix_core, mix_y, mix_send,
    rows_v, wts_v, hid_v, part_v, part_x, part_z, part_send,
    sh_v, sh_core, sh_y, sh_send,
    load_sem, halo_sem, z_send, z_recv, x_send, x_recv, y_send, y_recv, c_send, c_recv,
    w_send, w_recv, h_send, h_recv, rx_send, rx_recv, rz_send, rz_recv, m_send, m_recv,
):
    f32, bf16 = jnp.float32, jnp.bfloat16
    e = lax.axis_index("ep")
    t = lax.axis_index("tp")
    n_ep = Z_SIDE * X_SIDE
    z, x = e // X_SIDE, e % X_SIDE
    y, c = t // CORES, t % CORES
    toks = moe_h.shape[0]
    width = moe_h.shape[1]
    part = width // (Y_SIDE * CORES)
    hid = gate_h.shape[2]
    near = 2 * part // 8
    rest = part - near
    zs = [z, z + 1 - 2 * (z % 2), (z + 2) % 4, 3 - z]
    xs = [x, 1 - x]
    ty, tc, tyc = (1 - y) * CORES + c, y * CORES + 1 - c, (1 - y) * CORES + 1 - c

    def row0(k, j):
        return pl.multiple_of((zs[k] * X_SIDE + xs[j]) * toks, toks)

    def col(s, shift=0):
        return pl.multiple_of(s * part + shift, 128)

    loads = []
    for i, (src, dst) in enumerate((
        (moe_h, moe_v), (gain_h, gain_v), (pool_h, pool_v),
        (map_h.at[pl.ds(t * map_v.shape[0], map_v.shape[0])], map_v),
        (scale_h.at[:, pl.ds(pl.multiple_of(t * scale_v.shape[1], 128), scale_v.shape[1])], scale_v),
        (wt_h, wts_v.at[e]), (sg_h, sg_v), (su_h, su_v), (proj_h, proj_v),
        (gate_h.at[0], gate_v), (up_h.at[0], up_v), (sd_h, sd_v), (down_h.at[0], down_v),
    )):
        cp = pltpu.make_async_copy(src, dst, load_sem.at[i])
        cp.start()
        loads.append(cp)

    barrier = pltpu.get_barrier_semaphore()
    for k in range(Z_SIDE):
        for j in range(X_SIDE):
            if k or j:
                pl.semaphore_signal(barrier, inc=1, device_id={"ep": zs[k] * X_SIDE + xs[j], "tp": t},
                                    device_id_type=pl.DeviceIdType.MESH)
    for peer in (ty, tc):
        pl.semaphore_signal(barrier, inc=1, device_id={"ep": e, "tp": peer},
                            device_id_type=pl.DeviceIdType.MESH)
    pl.semaphore_wait(barrier, n_ep - 1 + 2)

    sent = []

    def push(src, dst, ssem, rsem, ep, tp):
        cp = pltpu.make_async_remote_copy(src_ref=src, dst_ref=dst, send_sem=ssem, recv_sem=rsem,
                                          device_id={"ep": ep, "tp": tp},
                                          device_id_type=pl.DeviceIdType.MESH)
        cp.start()
        sent.append(cp)

    def arrived(ref, ssem, rsem):
        pltpu.make_async_remote_copy(src_ref=ref, dst_ref=ref, send_sem=ssem, recv_sem=rsem,
                                     device_id={"ep": e, "tp": tc},
                                     device_id_type=pl.DeviceIdType.MESH).wait_recv()

    loads[0].wait()
    loads[1].wait()
    own = row0(0, 0)

    def norm_step(i, carry):
        r = pl.multiple_of(i * 16, 16)
        v = moe_v[pl.ds(r, 16), :].astype(f32)
        cen = v - jnp.mean(v, axis=1, keepdims=True)
        var = jnp.mean(cen * cen, axis=1, keepdims=True)
        rows_v[pl.ds(own + r, 16), :] = (cen * lax.rsqrt(var + eps) * gain_v[...]).astype(bf16)
        return carry

    lax.fori_loop(0, toks // 16, norm_step, 0)

    def primary(k, j):
        r = row0(k, j)
        return (rows_v.at[pl.ds(r, toks), pl.ds(col(t), part)],
                rows_v.at[pl.ds(r, toks), pl.ds(col(ty, near), rest)])

    inner = (z > 0) & (z < Z_SIDE - 1)
    handed = []

    def hops(k, to, at, slot):
        return [pltpu.make_async_remote_copy(
            src_ref=ref, dst_ref=ref, send_sem=z_send.at[slot, i], recv_sem=z_recv.at[at, i],
            device_id={"ep": zs[to] * X_SIDE + x, "tp": t}, device_id_type=pl.DeviceIdType.MESH)
            for i, ref in enumerate(primary(k, 0))]

    def hand(k, to, at, slot):
        handed.append((k, to, at, slot))
        for cp in hops(k, to, at, slot):
            cp.start()

    for cp in hops(0, 1, 1, 0):
        cp.start()
        sent.append(cp)

    @pl.when(inner)
    def _():
        hand(0, 3, 3, 1)

    for i, ref in enumerate(primary(0, 0)):
        push(ref, ref, x_send.at[0, i], x_recv.at[0, i], z * X_SIDE + xs[1], t)
    loads[5].wait()
    for k in range(Z_SIDE):
        for j in range(X_SIDE):
            if k or j:
                push(wts_v.at[e], wts_v.at[e], w_send.at[k, j], w_recv.at[k, j], zs[k] * X_SIDE + xs[j], t)

    def near_ref(k, j, s):
        return rows_v.at[pl.ds(row0(k, j), toks), pl.ds(col(s), near)]

    def z_wait(k):
        for i, ref in enumerate(primary(k, 0)):
            arrived(ref, z_send.at[k, i], z_recv.at[k, i])

    def z_arrive(k):
        if k < 3:
            z_wait(k)

            @pl.when(inner)
            def _():
                if k == 1:
                    hand(1, 3, 2, 2)
                    z_wait(3)
                    hand(3, 1, 2, 3)
                else:
                    hand(2, 1, 3, 4)
        else:
            @pl.when(jnp.logical_not(inner))
            def _():
                z_wait(3)

        for i, ref in enumerate(primary(k, 0)):
            push(ref, ref, x_send.at[k, i], x_recv.at[k, i], z * X_SIDE + xs[1], t)
        push(near_ref(k, 0, t), near_ref(k, 0, t), y_send.at[k, 0], y_recv.at[k, 0], e, ty)

    def x_arrive(k):
        for i, ref in enumerate(primary(k, 1)):
            arrived(ref, x_send.at[k, i], x_recv.at[k, i])
        push(near_ref(k, 1, t), near_ref(k, 1, t), y_send.at[k, 1], y_recv.at[k, 1], e, ty)

    def pair_ref(k, s):
        if k == 0:
            return rows_v.at[pl.ds(row0(0, 1), toks), pl.ds(col(s), part)]
        r = pl.multiple_of(zs[k] * X_SIDE * toks, toks)
        return rows_v.at[pl.ds(r, X_SIDE * toks), pl.ds(col(s), part)]

    def y_arrive(k):
        for j in (0, 1):
            if k or j:
                arrived(near_ref(k, j, ty), y_send.at[k, j], y_recv.at[k, j])
        for i, s in enumerate((t, ty)):
            push(pair_ref(k, s), pair_ref(k, s), c_send.at[k, i], c_recv.at[k, i], e, tc)

    def core_arrive(k):
        for i, s in enumerate((tc, tyc)):
            arrived(pair_ref(k, s), c_send.at[k, i], c_recv.at[k, i])

    def hid_ref(k, s):
        r = pl.multiple_of(zs[k] * X_SIDE * toks, toks)
        return hid_v.at[pl.ds(r, X_SIDE * toks), pl.ds(pl.multiple_of(s * hid, 128), hid)]

    def expert_in(k):
        r = pl.multiple_of(zs[k] * X_SIDE * toks, toks)
        rows = rows_v[pl.ds(r, X_SIDE * toks), :]
        g = jnp.dot(rows, gate_v[...], preferred_element_type=f32)
        u = jnp.dot(rows, up_v[...], preferred_element_type=f32)
        hid_ref(k, t)[...] = (g / (1.0 + jnp.exp(-g)) * u).astype(bf16)
        push(hid_ref(k, t), hid_ref(k, t), h_send.at[k, 0], h_recv.at[k, 0], e, ty)
        push(hid_ref(k, t), hid_ref(k, t), h_send.at[k, 1], h_recv.at[k, 1], e, tc)

    def hid_forward(k):
        arrived(hid_ref(k, ty), h_send.at[k, 0], h_recv.at[k, 0])
        push(hid_ref(k, ty), hid_ref(k, ty), h_send.at[k, 2], h_recv.at[k, 2], e, tc)

    def weight_col(k, j):
        b = zs[k] * X_SIDE + xs[j]
        row = wts_v[b, pl.ds(e, 1), :]
        a = lax.broadcasted_iota(jnp.int32, (toks, toks), 0)
        b2 = lax.broadcasted_iota(jnp.int32, (toks, toks), 1)
        return jnp.sum(jnp.where(a == b2, jnp.broadcast_to(row, (toks, toks)), 0.0), axis=1, keepdims=True)

    def expert_out(k):
        arrived(hid_ref(k, tc), h_send.at[k, 1], h_recv.at[k, 1])
        arrived(hid_ref(k, tyc), h_send.at[k, 2], h_recv.at[k, 2])
        for j in (1, 0):
            if k or j:
                b = zs[k] * X_SIDE + xs[j]
                arrived(wts_v.at[b], w_send.at[k, j], w_recv.at[k, j])
        for j in (1, 0):
            r = row0(k, j)
            wcol = weight_col(k, j)
            for q in range(part // 256):
                o = jnp.dot(hid_v[pl.ds(r, toks), :], down_v[:, q * 256:(q + 1) * 256],
                            preferred_element_type=f32)
                part_v[pl.ds(r, toks), q * 256:(q + 1) * 256] = (o.astype(bf16).astype(f32) * wcol).astype(bf16)
                if k == 3 and j == 1 and (q + 1) * 256 in (half, part):
                    half_push(k, (q + 1) * 256 // half - 1)

    half = part // 2

    def half_push(k, h):
        cols = pl.ds(h * half, half)
        push(part_v.at[pl.ds(row0(k, 1), toks), cols], part_x.at[k, :, cols], rx_send.at[k, h],
             rx_recv.at[k, h], z * X_SIDE + xs[1], t)

    def out_push(k):
        half_push(k, 0)
        half_push(k, 1)

    def sum_x(k):
        for h in (0, 1):
            cols = pl.ds(h * half, half)
            arrived(part_x.at[k, :, cols], rx_send.at[k, h], rx_recv.at[k, h])
            part_send[k, :, cols] = (part_v[pl.ds(row0(k, 0), toks), cols].astype(f32)
                                     + part_x[k, :, cols].astype(f32)).astype(bf16)
            if k:
                push(part_send.at[k, :, cols], part_z.at[k, :, cols], rz_send.at[k, h], rz_recv.at[k, h],
                     zs[k] * X_SIDE + x, t)

    loads[6].wait()
    loads[7].wait()
    rows = rows_v[pl.ds(own, toks), :]
    g = jnp.dot(rows, sg_v[...], preferred_element_type=f32)
    u = jnp.dot(rows, su_v[...], preferred_element_type=f32)
    shared_hidden = (g / (1.0 + jnp.exp(-g)) * u).astype(bf16)
    loads[11].wait()
    for q in range(width // 512):
        sh_v[:, q * 512:(q + 1) * 512] = jnp.dot(
            shared_hidden, sd_v[:, q * 512:(q + 1) * 512], preferred_element_type=f32).astype(bf16)
    for i, s in enumerate((tc, tyc)):
        push(sh_v.at[:, pl.ds(col(s), part)], sh_core.at[i], m_send.at[0, i], m_recv.at[0, i], e, tc)

    loads[2].wait()
    count = pool_v.shape[0]
    tail_ref = pool_v.at[pl.ds(count - HALO, HALO), :]

    def halo_copy(target):
        return pltpu.make_async_remote_copy(src_ref=tail_ref, dst_ref=halo_v, send_sem=halo_sem.at[0],
                                            recv_sem=halo_sem.at[1], device_id={"ep": target, "tp": t},
                                            device_id_type=pl.DeviceIdType.MESH)

    @pl.when(e < n_ep - 1)
    def _():
        halo_copy(e + 1).start()

    @pl.when(e == 0)
    def _():
        halo_v[...] = jnp.zeros_like(halo_v)

    @pl.when(e > 0)
    def _():
        halo_copy(e - 1).wait_recv()

    ext_v[:HALO, :] = halo_v[...].astype(f32)
    ext_v[HALO:, :] = pool_v[...].astype(f32)
    loads[3].wait()
    loads[4].wait()
    dim = map_v.shape[1]
    position = (e * count + lax.broadcasted_iota(jnp.int32, (count, dim), 0)).astype(f32)
    for grp in range(map_v.shape[0]):
        w = windows[grp % 4]
        cs = slice(grp * dim, (grp + 1) * dim)
        values = ext_v[HALO:, cs]
        running = values
        for lag in range(1, w):
            running = running + ext_v[HALO - lag:HALO - lag + count, cs]
        pooled = (running / jnp.minimum(position + 1.0, float(w)) - values).astype(bf16)
        mapped = jnp.dot(pooled, map_v[grp], preferred_element_type=f32)
        group_v[:, cs] = (mapped * scale_v[:, cs]).astype(bf16)
    loads[8].wait()

    def proj_step(q, carry):
        cq = pl.ds(pl.multiple_of(q * 512, 512), 512)
        mix_v[:, cq] = jnp.dot(group_v[...], proj_v[:, cq], preferred_element_type=f32).astype(bf16)
        return carry

    lax.fori_loop(0, width // 512, proj_step, 0)
    for i, s in enumerate((tc, tyc)):
        push(mix_v.at[:, pl.ds(col(s), part)], mix_core.at[i], m_send.at[1, i], m_recv.at[1, i], e, tc)

    def core_sum(which, own_ref, core_ref, send_ref, y_ref):
        for i in (0, 1):
            arrived(core_ref.at[i], m_send.at[which, i], m_recv.at[which, i])
        send_ref[...] = (own_ref[:, pl.ds(col(ty), part)].astype(f32) + core_ref[1].astype(f32)).astype(bf16)
        push(send_ref, y_ref, m_send.at[which, 2], m_recv.at[which, 2], e, ty)

    def y_sum(which, own_ref, core_ref, y_ref):
        arrived(y_ref, m_send.at[which, 2], m_recv.at[which, 2])
        return own_ref[:, pl.ds(col(t), part)].astype(f32) + core_ref[0].astype(f32) + y_ref[...].astype(f32)

    core_sum(0, sh_v, sh_core, sh_send, sh_y)
    z_arrive(1)
    x_arrive(0)
    y_arrive(0)
    core_arrive(0)
    loads[9].wait()
    loads[10].wait()
    expert_in(0)
    z_arrive(2)
    x_arrive(1)
    hid_forward(0)
    y_arrive(1)
    core_arrive(1)
    expert_in(1)
    loads[12].wait()
    expert_out(0)
    z_arrive(3)
    out_push(0)
    x_arrive(2)
    hid_forward(1)
    y_arrive(2)
    expert_out(1)
    out_push(1)
    core_arrive(2)
    expert_in(2)
    x_arrive(3)
    hid_forward(2)
    expert_out(2)
    out_push(2)
    y_arrive(3)
    sum_x(1)
    core_arrive(3)
    expert_in(3)
    core_sum(1, mix_v, mix_core, mix_send, mix_y)
    sum_x(2)
    hid_forward(3)
    expert_out(3)
    sum_x(0)
    total = y_sum(0, sh_v, sh_core, sh_y) + part_send[0].astype(f32)
    mix_out[...] = y_sum(1, mix_v, mix_core, mix_y).astype(bf16)
    sum_x(3)
    for k in (1, 2, 3):
        for h in (0, 1):
            arrived(part_z.at[k, :, pl.ds(h * half, half)], rz_send.at[k, h], rz_recv.at[k, h])
        total = total + part_z[k].astype(f32)
    moe_out[...] = total.astype(bf16)

    for cp in sent:
        cp.wait_send()

    @pl.when(inner)
    def _():
        for which in handed:
            for cp in hops(*which):
                cp.wait_send()

    @pl.when(e < n_ep - 1)
    def _():
        halo_copy(e + 1).wait_send()


def per_device_fused(
    pool_input, pool_map, pool_scale, out_proj, moe_input, norm_gain, routes, route_weights,
    expert_gate, expert_up, expert_down, shared_gate, shared_up, shared_down,
):
    f32, bf16 = jnp.float32, jnp.bfloat16
    n_ep = lax.axis_size("ep")
    toks, width = moe_input.shape
    count, channels = pool_input.shape
    dim = pool_map.shape[1]
    part = width // lax.axis_size("tp")
    ids = jnp.arange(n_ep, dtype=jnp.int32)
    weights = jnp.sum(
        jnp.where(routes[None, :, :] == ids[:, None, None], route_weights[None, :, :], 0.0), axis=2)
    dma = pltpu.SemaphoreType.DMA
    return pl.pallas_call(
        fused_kernel,
        out_shape=(jax.ShapeDtypeStruct((count, part), bf16), jax.ShapeDtypeStruct((toks, part), bf16)),
        in_specs=[pl.BlockSpec(memory_space=pl.ANY)] * 13,
        out_specs=(pl.BlockSpec(memory_space=pltpu.VMEM), pl.BlockSpec(memory_space=pltpu.VMEM)),
        scratch_shapes=[
            pltpu.VMEM((count, channels), bf16),
            pltpu.VMEM((channels // dim, dim, dim), bf16),
            pltpu.VMEM((1, channels), f32),
            pltpu.VMEM(out_proj.shape, bf16),
            pltpu.VMEM((toks, width), bf16),
            pltpu.VMEM((1, width), f32),
            pltpu.VMEM(expert_gate.shape[1:], bf16),
            pltpu.VMEM(expert_up.shape[1:], bf16),
            pltpu.VMEM(expert_down.shape[1:], bf16),
            pltpu.VMEM(shared_gate.shape, bf16),
            pltpu.VMEM(shared_up.shape, bf16),
            pltpu.VMEM(shared_down.shape, bf16),
            pltpu.VMEM((HALO, channels), bf16),
            pltpu.VMEM((HALO + count, channels), f32),
            pltpu.VMEM((count, channels), bf16),
            pltpu.VMEM((count, width), bf16),
            pltpu.VMEM((2, count, part), bf16),
            pltpu.VMEM((count, part), bf16),
            pltpu.VMEM((count, part), bf16),
            pltpu.VMEM((n_ep * toks, width), bf16),
            pltpu.VMEM((n_ep, n_ep, toks), f32),
            pltpu.VMEM((n_ep * toks, expert_down.shape[1]), bf16),
            pltpu.VMEM((n_ep * toks, part), bf16),
            pltpu.VMEM((Z_SIDE, toks, part), bf16),
            pltpu.VMEM((Z_SIDE, toks, part), bf16),
            pltpu.VMEM((Z_SIDE, toks, part), bf16),
            pltpu.VMEM((toks, width), bf16),
            pltpu.VMEM((2, toks, part), bf16),
            pltpu.VMEM((toks, part), bf16),
            pltpu.VMEM((toks, part), bf16),
            dma((13,)), dma((2,)),
            dma((5, 2)), dma((4, 2)), dma((4, 2)), dma((4, 2)), dma((4, 2)), dma((4, 2)),
            dma((4, 2)), dma((4, 2)), dma((4, 2)), dma((4, 2)), dma((4, 3)), dma((4, 3)),
            dma((4, 2)), dma((4, 2)), dma((4, 2)), dma((4, 2)), dma((2, 3)), dma((2, 3)),
        ],
        compiler_params=pltpu.CompilerParams(
            collective_id=0, has_side_effects=True, vmem_limit_bytes=60 * 1024 * 1024),
    )(
        pool_input, pool_map, pool_scale.reshape(1, -1), out_proj, moe_input, norm_gain.reshape(1, -1),
        weights, expert_gate, expert_up, expert_down, shared_gate, shared_up, shared_down,
    )


def solution(mesh):
    plane = mesh.shape["ep"] == Z_SIDE * X_SIDE and mesh.shape["tp"] == Y_SIDE * CORES
    body = per_device_fused if plane else per_device
    return jax.shard_map(
        body,
        mesh=mesh,
        in_specs=(
            P("ep", "tp"),
            P(),
            P(),
            P("tp", None),
            P("ep", None),
            P(),
            P("ep", None),
            P("ep", None),
            P("ep", None, "tp"),
            P("ep", None, "tp"),
            P("ep", None, "tp"),
            P(None, "tp"),
            P(None, "tp"),
            P("tp", None),
        ),
        out_specs=(P("ep", "tp"), P("ep", "tp")),
        check_vma=False,
    )
```

profile of v0, /device:TPU:0, one launch (start us, length us, event | category | flops | bytes accessed | tf_op | source)
XLA Modules:
  0.0 100.8 jit_solution(3364637372272485529)
XLA Ops:
  0.6 1.3 %select_reduce_fusion.wt_h = f32[8,128]{1,0:T(8,128)} fusion(f32[128,4]{0,1:T(4,128)} %param.21, s32[128,4]{0,1:T(4,128)} %param.20), kind=kLoop, calls=%fused_computation | loop fusion | flops 11264 | bytes 8192 | tf_op jit(solution)/shard_map/reduce_sum | solution.py:512
  1.9 95.3 %shard_map.149 = (bf16[256,1024]{1,0:T(8,128)(2,1)}, bf16[128,1024]{1,0:T(8,128)(2,1)}) custom-call(bf16[256,512]{1,0:T(8,128)(2,1)} %pool_h.1, bf16[16,128,128]{2,1,0:T(8,128)(2,1)} %map_h.1, f32[1,2048]{1,0:T(1,128)} %bitcast.3, bf16[512,4096]{1,0:T(8,128)(2,1)} %proj_h.1, bf16[128,4096]{1,0:T(8,128)(2,1)} %moe_h.1, f32[1,4096]{1,0:T(1,128)} %bitcast.2, ...), custom_call_target="tpu_custom_call" | custom-call | tf_op jit(solution)/shard_map/pallas_call | solution.py:515
  97.3 1.9 %copy.20 = bf16[256,1024]{1,0:T(8,128)(2,1)} copy(bf16[256,1024]{1,0:T(8,128)(2,1)} %get-tuple-element.4) | data formatting | bytes 1048576
  99.1 1.7 %copy.21 = bf16[128,1024]{1,0:T(8,128)(2,1)} copy(bf16[128,1024]{1,0:T(8,128)(2,1)} %get-tuple-element.5) | data formatting | bytes 524288
where the time goes:
time: 102 us; the launch traced here: 101 us
  Pallas kernels  95.3 us (93%)
  local copies, waits for them, and re-layouts  3.54 us (3%)
  other arithmetic  1.3 us (1%)
    pallas_call x1, Pallas kernels, per_device_fused(): pl.pallas_call(fused_kernel, out_shape=(jax.ShapeDtypeStruct((count, part...  95.3 us
    unnamed x2, local copies, waits for them, and re-layouts  3.54 us

commit v1 on v0

v1 whole, which is shorter than its diff:
```python
import jax
import jax.numpy as jnp
from jax import lax
from jax.experimental import pallas as pl
from jax.experimental.pallas import tpu as pltpu
from jax.sharding import PartitionSpec as P

windows = (2, 4, 8, 16)
reach_back = 15
eps = 1e-05


def passed_along(block, axis, distance):
    devices = range(lax.axis_size(axis))
    route = [(i - distance, i) for i in devices if i - distance in devices]
    return lax.ppermute(block, axis, route)


def pool_branch(pool_input, pool_map, pool_scale, out_proj):
    row_count = pool_input.shape[0]
    channels = pool_input.shape[1]
    group_dim = pool_map.shape[1]
    local_groups = channels // group_dim
    tp_rank = lax.axis_index("tp")
    ep_rank = lax.axis_index("ep")
    earlier_rows = passed_along(pool_input[row_count - reach_back :], "ep", 1)
    values = pool_input.astype(jnp.float32)
    extended = jnp.concatenate([earlier_rows.astype(jnp.float32), values], axis=0)
    position = (ep_rank * row_count + jnp.arange(row_count, dtype=jnp.int32)).astype(jnp.float32)
    group_ids = tp_rank * local_groups + jnp.arange(channels, dtype=jnp.int32) // group_dim
    group_kind = group_ids % 4
    running = jnp.zeros((row_count, channels), jnp.float32)
    pooled = -values
    for lag_step in range(reach_back + 1):
        running = running + extended[reach_back - lag_step : reach_back - lag_step + row_count]
        if lag_step + 1 in windows:
            kind_id = windows.index(lag_step + 1)
            counts = jnp.minimum(position + 1.0, float(lag_step + 1))
            select = (group_kind == kind_id).astype(jnp.float32)
            pooled = pooled + select[None, :] * running / counts[:, None]
    pooled = pooled.astype(jnp.bfloat16)
    my_maps = lax.dynamic_slice_in_dim(pool_map, tp_rank * local_groups, local_groups, 0)
    my_scale = lax.dynamic_slice_in_dim(pool_scale, tp_rank * channels, channels, 0)
    mapped = jnp.einsum(
        "rgc,gcd->rgd",
        pooled.reshape(row_count, local_groups, group_dim),
        my_maps,
        preferred_element_type=jnp.float32,
    )
    group_out = (mapped.reshape(row_count, channels) * my_scale[None, :]).astype(jnp.bfloat16)
    return jnp.dot(group_out, out_proj, preferred_element_type=jnp.float32)


def dispatch_rows(routes, expert_count, capacity):
    tok_count, top_count = routes.shape
    flat_ids = routes.reshape(tok_count * top_count)
    one_hot = (flat_ids[:, None] == jnp.arange(expert_count, dtype=jnp.int32)[None, :]).astype(
        jnp.int32
    )
    earlier = jnp.cumsum(one_hot, axis=0) - one_hot
    slot_ids = jnp.sum(earlier * one_hot, axis=1)
    return (flat_ids * capacity + slot_ids).reshape(tok_count, top_count)


def per_device(
    pool_input,
    pool_map,
    pool_scale,
    out_proj,
    moe_input,
    norm_gain,
    routes,
    route_weights,
    expert_gate,
    expert_up,
    expert_down,
    shared_gate,
    shared_up,
    shared_down,
):
    mixer_part = pool_branch(pool_input, pool_map, pool_scale, out_proj)
    values = moe_input.astype(jnp.float32)
    centre = values - jnp.mean(values, axis=1, keepdims=True)
    variance = jnp.mean(centre * centre, axis=1, keepdims=True)
    normed = (centre * lax.rsqrt(variance + eps) * norm_gain[None, :]).astype(jnp.bfloat16)
    expert_count = lax.axis_size("ep")
    tok_count = moe_input.shape[0]
    top_count = routes.shape[1]
    capacity = (3 * tok_count * top_count + 2 * expert_count - 1) // (2 * expert_count)
    slot_index = dispatch_rows(routes, expert_count, capacity)
    buffer_len = expert_count * capacity
    targets = jnp.arange(buffer_len, dtype=jnp.int32)[:, None]
    placing = jnp.zeros((buffer_len, tok_count), jnp.float32)
    for top_step in range(top_count):
        placing = placing + (targets == slot_index[None, :, top_step]).astype(jnp.float32)
    outgoing = jnp.dot(
        placing.astype(jnp.bfloat16), normed, preferred_element_type=jnp.float32
    ).astype(jnp.bfloat16)
    gate_weight = expert_gate[0]
    up_weight = expert_up[0]
    down_weight = expert_down[0]
    tp_rank = lax.axis_index("tp")
    slice_width = outgoing.shape[1] // lax.axis_size("tp")
    my_slice = lax.dynamic_slice_in_dim(outgoing, tp_rank * slice_width, slice_width, 1)
    arrived = lax.all_to_all(my_slice, "ep", split_axis=0, concat_axis=0, tiled=True)
    shard_cols = lax.all_gather(arrived, "tp", axis=1, tiled=True)
    gate_val = jnp.dot(shard_cols, gate_weight, preferred_element_type=jnp.float32)
    up_val = jnp.dot(shard_cols, up_weight, preferred_element_type=jnp.float32)
    hidden = (jax.nn.silu(gate_val) * up_val).astype(jnp.bfloat16)
    expert_result = jnp.dot(
        lax.all_gather(hidden, "tp", axis=1, tiled=True),
        down_weight,
        preferred_element_type=jnp.float32,
    ).astype(jnp.bfloat16)
    returned = lax.all_to_all(expert_result, "ep", split_axis=0, concat_axis=0, tiled=True)
    routed = jnp.zeros((tok_count, returned.shape[1]), jnp.float32)
    for top_step in range(top_count):
        picked = returned[slot_index[:, top_step]].astype(jnp.float32)
        routed = routed + route_weights[:, top_step, None] * picked
    shared_gate_val = jnp.dot(normed, shared_gate, preferred_element_type=jnp.float32)
    shared_up_val = jnp.dot(normed, shared_up, preferred_element_type=jnp.float32)
    shared_hidden = (jax.nn.silu(shared_gate_val) * shared_up_val).astype(jnp.bfloat16)
    shared_part = jnp.dot(shared_hidden, shared_down, preferred_element_type=jnp.float32)
    mixer_sum, shared_sum = (
        lax.psum_scatter(
            mixer_part.astype(jnp.bfloat16), "tp", scatter_dimension=1, tiled=True
        ).astype(jnp.float32),
        lax.psum_scatter(
            shared_part.astype(jnp.bfloat16), "tp", scatter_dimension=1, tiled=True
        ).astype(jnp.float32),
    )
    return (mixer_sum.astype(jnp.bfloat16), (routed + shared_sum).astype(jnp.bfloat16))


HALO = 16
Z_SIDE, X_SIDE, Y_SIDE, CORES = 4, 2, 2, 2
MIX_PARTS = 4


def fused_kernel(
    pool_h, map_h, scale_h, proj_h, moe_h, gain_h, route_h, rw_h, gate_h, up_h, down_h, sg_h, su_h, sd_h,
    mix_out, moe_out,
    pool_v, map_v, scale_v, proj_v, moe_v, gain_v, route_v, rw_v, gate_v, up_v, down_v, sg_v, su_v, sd_v,
    halo_v, ext_v, group_v, mix_v, mix_core, mix_y, mix_send,
    raw_v, comp_v, xs_v, wts_v, slot_v, pick_v, mixw_v, hid_v, outx_v, pair_v, acc_v, part_z, part_send,
    sh_v, sh_core, sh_y, sh_send,
    load_sem, halo_sem, z_send, z_recv, x_send, x_recv, y_send, y_recv, c_send, c_recv,
    w_send, w_recv, h_send, h_recv, rx_send, rx_recv, rz_send, rz_recv, m_send, m_recv, ms_send, ms_recv,
):
    f32, bf16 = jnp.float32, jnp.bfloat16
    e = lax.axis_index("ep")
    t = lax.axis_index("tp")
    n_ep = Z_SIDE * X_SIDE
    z, x = e // X_SIDE, e % X_SIDE
    y, c = t // CORES, t % CORES
    toks = moe_h.shape[0]
    width = moe_h.shape[1]
    cap = comp_v.shape[0] // n_ep
    part = width // (Y_SIDE * CORES)
    hid = gate_h.shape[2]
    near = NEAR * part // 8
    rest = part - near
    inner = (z > 0) & (z < Z_SIDE - 1)
    kin = [z, z + 1 - 2 * (z % 2), (z + 2) % 4, 3 - z]
    turn = [0, jnp.where(inner, 3, 1), 2, jnp.where(inner, 1, 3)]
    zs = [z, jnp.where(inner, kin[3], kin[1]), kin[2], jnp.where(inner, kin[1], kin[3])]
    xs = [x, 1 - x]
    ex = z * X_SIDE + xs[1]
    ty, tc, tyc = (1 - y) * CORES + c, y * CORES + 1 - c, (1 - y) * CORES + 1 - c

    barrier = pltpu.get_barrier_semaphore()
    for k in range(Z_SIDE):
        for j in range(X_SIDE):
            if k or j:
                pl.semaphore_signal(barrier, inc=1, device_id={"ep": zs[k] * X_SIDE + xs[j], "tp": t},
                                    device_id_type=pl.DeviceIdType.MESH)
    for peer in (ty, tc):
        pl.semaphore_signal(barrier, inc=1, device_id={"ep": e, "tp": peer},
                            device_id_type=pl.DeviceIdType.MESH)

    def raw_row(k):
        return pl.multiple_of(zs[k] * toks, toks)

    def row0(k, j):
        return pl.multiple_of((zs[k] * X_SIDE + xs[j]) * cap, cap)

    def pair_row(k):
        return pl.multiple_of(zs[k] * X_SIDE * cap, X_SIDE * cap)

    def col(s, shift=0):
        return pl.multiple_of(s * part + shift, 128)

    loads = {}
    for i, (name, src, dst) in enumerate((
        ("moe", moe_h, moe_v), ("gain", gain_h, gain_v),
        ("route", route_h, route_v), ("rw", rw_h, rw_v), ("pool", pool_h, pool_v),
        ("map", map_h.at[pl.ds(t * map_v.shape[0], map_v.shape[0])], map_v),
        ("scale", scale_h.at[:, pl.ds(pl.multiple_of(t * scale_v.shape[1], 128), scale_v.shape[1])], scale_v),
        ("sg", sg_h, sg_v), ("su", su_h, su_v), ("sd", sd_h, sd_v), ("proj", proj_h, proj_v),
        ("gate", gate_h.at[0], gate_v), ("up", up_h.at[0], up_v), ("down", down_h.at[0], down_v),
    )):
        cp = pltpu.make_async_copy(src, dst, load_sem.at[i])
        cp.start()
        loads[name] = cp

    sent = []

    def remote(src, dst, ssem, rsem, ep, tp):
        return pltpu.make_async_remote_copy(src_ref=src, dst_ref=dst, send_sem=ssem, recv_sem=rsem,
                                            device_id={"ep": ep, "tp": tp},
                                            device_id_type=pl.DeviceIdType.MESH)

    def start(cp):
        cp.start()
        sent.append(cp)

    def push(src, dst, ssem, rsem, ep, tp):
        start(remote(src, dst, ssem, rsem, ep, tp))

    def arrived(ref, ssem, rsem):
        pltpu.make_async_remote_copy(src_ref=ref, dst_ref=ref, send_sem=ssem, recv_sem=rsem,
                                     device_id={"ep": e, "tp": tc},
                                     device_id_type=pl.DeviceIdType.MESH).wait_recv()

    def routing(k):
        w = wts_v[k]
        a = lax.broadcasted_iota(jnp.int32, (toks, toks), 0)
        b = lax.broadcasted_iota(jnp.int32, (toks, toks), 1)
        before = jnp.where(a < b, 1.0, 0.0).astype(bf16)
        slot = jnp.dot(jnp.where(w > 0.0, 1.0, 0.0).astype(bf16), before, preferred_element_type=f32)
        slot_v[k] = jnp.where(w > 0.0, slot, -1024.0)
        own_row, other_row = slot_v[k, pl.ds(e, 1), :], slot_v[k, pl.ds(ex, 1), :]
        r = lax.broadcasted_iota(jnp.int32, (X_SIDE * cap, toks), 0).astype(f32)
        place = jnp.where(r < float(cap), jnp.broadcast_to(own_row, r.shape),
                          jnp.broadcast_to(other_row, r.shape) + float(cap))
        pick_v[k] = jnp.where(place == r, 1.0, 0.0).astype(bf16)

        def turned(row):
            return jnp.sum(jnp.where(a == b, jnp.broadcast_to(row, (toks, toks)), 0.0), axis=1, keepdims=True)

        s = lax.broadcasted_iota(jnp.int32, (toks, X_SIDE * cap), 1).astype(f32)
        first = s < float(cap)
        place = jnp.where(first, turned(own_row), turned(other_row) + float(cap))
        value = jnp.where(first, turned(wts_v[k, pl.ds(e, 1), :]), turned(wts_v[k, pl.ds(ex, 1), :]))
        mixw_v[k] = jnp.where(place == s, value, 0.0).astype(bf16)

    loads["moe"].wait()
    loads["gain"].wait()
    own = raw_row(0)

    def norm_step(i, carry):
        r = pl.multiple_of(i * 16, 16)
        v = moe_v[pl.ds(r, 16), :].astype(f32)
        cen = v - jnp.mean(v, axis=1, keepdims=True)
        var = jnp.mean(cen * cen, axis=1, keepdims=True)
        raw_v[pl.ds(own + r, 16), :] = (cen * lax.rsqrt(var + eps) * gain_v[...]).astype(bf16)
        return carry

    lax.fori_loop(0, toks // 16, norm_step, 0, unroll=2)
    loads["pool"].wait()
    loads["route"].wait()
    loads["rw"].wait()
    ids = lax.broadcasted_iota(jnp.int32, (n_ep, toks), 0)
    weights = jnp.zeros((n_ep, toks), f32)
    for top_step in range(route_v.shape[0]):
        named = jnp.broadcast_to(route_v[top_step:top_step + 1, :], (n_ep, toks)) == ids
        weights = weights + jnp.where(named, jnp.broadcast_to(rw_v[top_step:top_step + 1, :], (n_ep, toks)), 0.0)
    wts_v[0] = weights

    pl.semaphore_wait(barrier, n_ep - 1 + 2)

    for k in range(1, Z_SIDE):
        push(wts_v.at[0], wts_v.at[k], w_send.at[k], w_recv.at[k], kin[k] * X_SIDE + x, t)

    count = pool_v.shape[0]
    tail_ref = pool_v.at[pl.ds(count - HALO, HALO), :]

    def halo_copy(target):
        return pltpu.make_async_remote_copy(src_ref=tail_ref, dst_ref=halo_v, send_sem=halo_sem.at[0],
                                            recv_sem=halo_sem.at[1], device_id={"ep": target, "tp": t},
                                            device_id_type=pl.DeviceIdType.MESH)

    @pl.when(e < n_ep - 1)
    def _():
        halo_copy(e + 1).start()

    def spans():
        return ((col(t), part), (col(ty, near), rest))

    def raw_ref(k, i):
        c0, n = spans()[i]
        return raw_v.at[pl.ds(pl.multiple_of(kin[k] * toks, toks), toks), pl.ds(c0, n)]

    handed = []

    def hop(k, to, at, slot, i):
        return pltpu.make_async_remote_copy(
            src_ref=raw_ref(k, i), dst_ref=raw_ref(k, i), send_sem=z_send.at[slot, i], recv_sem=z_recv.at[at, i],
            device_id={"ep": kin[to] * X_SIDE + x, "tp": t}, device_id_type=pl.DeviceIdType.MESH)

    def hand(k, to, at, slot, i):
        handed.append((k, to, at, slot, i))
        hop(k, to, at, slot, i).start()

    for i in (0, 1):
        cp = hop(0, 1, 1, 0, i)
        cp.start()
        sent.append(cp)

        @pl.when(inner)
        def _():
            hand(0, 3, 3, 1, i)

    step = 256

    def gather(k, i):
        c0, n = spans()[i]
        for q in range(n // step):
            cq = pl.ds(pl.multiple_of(c0 + q * step, 128), step)
            o = jnp.dot(pick_v[turn[k]], raw_v[pl.ds(raw_row(k), toks), cq], preferred_element_type=f32).astype(bf16)
            comp_v[pl.ds(row0(k, 0), cap), cq] = o[:cap]
            xs_v[k * cap:(k + 1) * cap, cq] = o[cap:]

    def x_copy(k, i):
        c0, n = spans()[i]
        return remote(xs_v.at[k * cap:(k + 1) * cap, pl.ds(c0, n)], comp_v.at[pl.ds(row0(k, 0), cap), pl.ds(c0, n)],
                      x_send.at[k, i], x_recv.at[k, i], ex, t)

    def x_push(k, i):
        start(x_copy(k, i))

    def near_ref(k, j, s):
        return comp_v.at[pl.ds(row0(k, j), cap), pl.ds(col(s), near)]

    def near_copy(k, j):
        return remote(near_ref(k, j, t), near_ref(k, j, t), y_send.at[k, j], y_recv.at[k, j], e, ty)

    def near_push(k, j):
        start(near_copy(k, j))

    routing(0)
    for i in (0, 1):
        gather(0, i)
        x_push(0, i)

    def gather_rest(c0, n):
        for q in range(n // step):
            cq = pl.ds(pl.multiple_of(c0 + q * step, 128), step)
            comp_v[pl.ds(row0(0, 0), cap), cq] = jnp.dot(
                pick_v[0, :cap], raw_v[pl.ds(own, toks), cq], preferred_element_type=f32).astype(bf16)

    gather_rest(col(ty), near)
    gather_rest(col(tc), part)
    gather_rest(col(tyc), part)

    def z_wait(k, i):
        arrived(raw_ref(k, i), z_send.at[k, i], z_recv.at[k, i])

    def w_arrive(k):
        arrived(wts_v.at[k], w_send.at[k], w_recv.at[k])
        routing(k)

    def rows_out(k, i):
        go = start if k < 3 else lambda cp: cp.start()
        gather(k, i)
        go(x_copy(k, i))
        if i == 0:
            go(near_copy(k, 0))

    def z_piece(k, i):
        if k < 3:
            z_wait(k, i)

            @pl.when(inner)
            def _():
                if k == 1:
                    hand(1, 3, 2, 2, i)
                    z_wait(3, i)
                    hand(3, 1, 2, 3, i)
                else:
                    hand(2, 1, 3, 4, i)

            rows_out(k, i)
        else:
            z_wait(3, i)
            rows_out(k, i)

    def early():
        @pl.when(inner)
        def _():
            for i in (0, 1):
                rows_out(3, i)

    def late(i):
        @pl.when(jnp.logical_not(inner))
        def _():
            z_piece(3, i)

    def x_piece(k, i):
        c0, n = spans()[i]
        arrived(comp_v.at[pl.ds(row0(k, 1), cap), pl.ds(c0, n)], x_send.at[k, i], x_recv.at[k, i])
        if i == 0:
            near_push(k, 1)

    def pair_ref(k, s):
        if k == 0:
            return comp_v.at[pl.ds(row0(0, 1), cap), pl.ds(col(s), part)]
        return comp_v.at[pl.ds(pair_row(k), X_SIDE * cap), pl.ds(col(s), part)]

    def y_arrive(k):
        for j in (0, 1):
            if k or j:
                arrived(near_ref(k, j, ty), y_send.at[k, j], y_recv.at[k, j])
        for i, s in enumerate((t, ty)):
            push(pair_ref(k, s), pair_ref(k, s), c_send.at[k, i], c_recv.at[k, i], e, tc)

    def core_arrive(k):
        for i, s in enumerate((tc, tyc)):
            arrived(pair_ref(k, s), c_send.at[k, i], c_recv.at[k, i])

    def hid_ref(k, s):
        return hid_v.at[pl.ds(pair_row(k), X_SIDE * cap), pl.ds(pl.multiple_of(s * hid, 128), hid)]

    def expert_in(k):
        rows = comp_v[pl.ds(pair_row(k), X_SIDE * cap), :]
        g = jnp.dot(rows, gate_v[...], preferred_element_type=f32)
        u = jnp.dot(rows, up_v[...], preferred_element_type=f32)
        hid_ref(k, t)[...] = (g / (1.0 + jnp.exp(-g)) * u).astype(bf16)
        push(hid_ref(k, t), hid_ref(k, t), h_send.at[k, 0], h_recv.at[k, 0], e, ty)
        push(hid_ref(k, t), hid_ref(k, t), h_send.at[k, 1], h_recv.at[k, 1], e, tc)

    def hid_forward(k):
        arrived(hid_ref(k, ty), h_send.at[k, 0], h_recv.at[k, 0])
        push(hid_ref(k, ty), hid_ref(k, ty), h_send.at[k, 2], h_recv.at[k, 2], e, tc)

    half = part // 2

    def half_push(k, h):
        cols = pl.ds(h * half, half)
        push(outx_v.at[k, :, cols], pair_v.at[k, pl.ds(cap, cap), cols], rx_send.at[k, h],
             rx_recv.at[k, h], ex, t)

    def out_push(k):
        half_push(k, 0)
        half_push(k, 1)

    def expert_out(k, send=True):
        arrived(hid_ref(k, tc), h_send.at[k, 1], h_recv.at[k, 1])
        arrived(hid_ref(k, tyc), h_send.at[k, 2], h_recv.at[k, 2])
        for j in (1, 0):
            rows = hid_v[pl.ds(row0(k, j), cap), :]
            for q in range(part // 256):
                o = jnp.dot(rows, down_v[:, q * 256:(q + 1) * 256], preferred_element_type=f32).astype(bf16)
                if j:
                    outx_v[k, :, q * 256:(q + 1) * 256] = o
                    if send and (q + 1) * 256 % half == 0:
                        half_push(k, (q + 1) * 256 // half - 1)
                else:
                    pair_v[k, :cap, q * 256:(q + 1) * 256] = o

    def sum_x(k):
        for h in (0, 1):
            cols = pl.ds(h * half, half)
            arrived(pair_v.at[k, pl.ds(cap, cap), cols], rx_send.at[k, h], rx_recv.at[k, h])
            both = jnp.dot(mixw_v[turn[k]], pair_v[k, :, cols], preferred_element_type=f32)
            if k:
                part_send[k, :, cols] = both.astype(bf16)
                push(part_send.at[k, :, cols], part_z.at[turn[k], :, cols], rz_send.at[k, h],
                     rz_recv.at[turn[k], h], zs[k] * X_SIDE + x, t)
            else:
                acc_v[:, cols] = both

    def shared():
        loads["sg"].wait()
        loads["su"].wait()
        rows = raw_v[pl.ds(own, toks), :]
        g = jnp.dot(rows, sg_v[...], preferred_element_type=f32)
        u = jnp.dot(rows, su_v[...], preferred_element_type=f32)
        shared_hidden = (g / (1.0 + jnp.exp(-g)) * u).astype(bf16)
        loads["sd"].wait()
        for q in range(width // 512):
            sh_v[:, q * 512:(q + 1) * 512] = jnp.dot(
                shared_hidden, sd_v[:, q * 512:(q + 1) * 512], preferred_element_type=f32).astype(bf16)
        for i, s in enumerate((tc, tyc)):
            push(sh_v.at[:, pl.ds(col(s), part)], sh_core.at[i], m_send.at[0, i], m_recv.at[0, i], e, tc)

    def pool():
        @pl.when(e == 0)
        def _():
            halo_v[...] = jnp.zeros_like(halo_v)

        @pl.when(e > 0)
        def _():
            halo_copy(e - 1).wait_recv()

        ext_v[:HALO, :] = halo_v[...].astype(f32)
        ext_v[HALO:, :] = pool_v[...].astype(f32)
        loads["map"].wait()
        loads["scale"].wait()
        dim = map_v.shape[1]
        position = (e * count + lax.broadcasted_iota(jnp.int32, (count, dim), 0)).astype(f32)
        for grp in range(map_v.shape[0]):
            w = windows[grp % 4]
            cs = slice(grp * dim, (grp + 1) * dim)
            values = ext_v[HALO:, cs]
            running = values
            for lag in range(1, w):
                running = running + ext_v[HALO - lag:HALO - lag + count, cs]
            pooled = (running / jnp.minimum(position + 1.0, float(w)) - values).astype(bf16)
            mapped = jnp.dot(pooled, map_v[grp], preferred_element_type=f32)
            group_v[:, cs] = (mapped * scale_v[:, cs]).astype(bf16)

    def proj():
        loads["proj"].wait()

        def proj_step(q, carry):
            cq = pl.ds(pl.multiple_of(q * 512, 512), 512)
            mix_v[:, cq] = jnp.dot(group_v[...], proj_v[:, cq], preferred_element_type=f32).astype(bf16)
            return carry

        lax.fori_loop(0, width // 512, proj_step, 0)
        for i, s in enumerate((tc, tyc)):
            push(mix_v.at[:, pl.ds(col(s), part)], mix_core.at[i], m_send.at[1, i], m_recv.at[1, i], e, tc)

    def core_sum(which, own_ref, core_ref, send_ref):
        for i in (0, 1):
            arrived(core_ref.at[i], m_send.at[which, i], m_recv.at[which, i])
        send_ref[...] = (own_ref[:, pl.ds(col(ty), part)].astype(f32) + core_ref[1].astype(f32)).astype(bf16)

    def sh_core_sum():
        core_sum(0, sh_v, sh_core, sh_send)

    def sh_push():
        push(sh_send, sh_y, m_send.at[0, 2], m_recv.at[0, 2], e, ty)

    def mix_core_sum():
        core_sum(1, mix_v, mix_core, mix_send)

    piece = count // MIX_PARTS

    def mix_push(n):
        push(mix_send.at[pl.ds(n * piece, piece)], mix_y.at[pl.ds(n * piece, piece)], ms_send.at[n], ms_recv.at[n],
             e, ty)

    def mix_final():
        for n in range(MIX_PARTS):
            arrived(mix_y.at[pl.ds(n * piece, piece)], ms_send.at[n], ms_recv.at[n])
        mix_out[...] = (mix_v[:, pl.ds(col(t), part)].astype(f32) + mix_core[0].astype(f32)
                        + mix_y[...].astype(f32)).astype(bf16)

    def sh_final():
        arrived(sh_y, m_send.at[0, 2], m_recv.at[0, 2])
        acc_v[...] = (acc_v[...] + sh_v[:, pl.ds(col(t), part)].astype(f32) + sh_core[0].astype(f32)
                      + sh_y[...].astype(f32))

    def z_final(h):
        cols = pl.ds(h * half, half)
        total = acc_v[:, cols]
        for k in (1, 2, 3):
            arrived(part_z.at[k, :, cols], rz_send.at[k, h], rz_recv.at[k, h])
            total = total + part_z[k, :, cols].astype(f32)
        moe_out[:, cols] = total.astype(bf16)

    def experts_loaded():
        loads["gate"].wait()
        loads["up"].wait()

    shared()
    w_arrive(1)
    w_arrive(2)
    w_arrive(3)
    pool()
    sh_core_sum()
    proj()
    x_piece(0, 0)
    mix_core_sum()
    z_piece(1, 0)
    x_piece(0, 1)
    z_piece(1, 1)
    y_arrive(0)
    x_piece(1, 0)
    core_arrive(0)
    experts_loaded()
    expert_in(0)
    z_piece(2, 0)
    x_piece(1, 1)
    y_arrive(1)
    core_arrive(1)
    expert_in(1)
    z_piece(2, 1)
    early()
    hid_forward(0)
    x_piece(2, 0)
    loads["down"].wait()
    expert_out(0, False)
    hid_forward(1)
    x_piece(2, 1)
    y_arrive(2)
    late(0)
    expert_out(1, False)
    core_arrive(2)
    expert_in(2)
    late(1)
    out_push(1)
    x_piece(3, 0)
    hid_forward(2)
    x_piece(3, 1)
    y_arrive(3)
    expert_out(2)
    core_arrive(3)
    expert_in(3)
    sh_push()
    mix_push(0)
    mix_push(1)
    mix_push(2)
    mix_push(3)
    sum_x(1)
    hid_forward(3)
    sum_x(2)
    expert_out(3)
    out_push(0)
    sum_x(3)
    sum_x(0)
    sh_final()
    mix_final()
    z_final(0)
    z_final(1)

    for cp in sent:
        cp.wait_send()
    for i in (0, 1):
        x_copy(3, i).wait_send()
    near_copy(3, 0).wait_send()

    @pl.when(inner)
    def _():
        for which in handed:
            hop(*which).wait_send()

    @pl.when(e < n_ep - 1)
    def _():
        halo_copy(e + 1).wait_send()


NEAR = 2


def per_device_fused(
    pool_input, pool_map, pool_scale, out_proj, moe_input, norm_gain, routes, route_weights,
    expert_gate, expert_up, expert_down, shared_gate, shared_up, shared_down,
):
    f32, bf16 = jnp.float32, jnp.bfloat16
    n_ep = lax.axis_size("ep")
    toks, width = moe_input.shape
    top_count = routes.shape[1]
    count, channels = pool_input.shape
    dim = pool_map.shape[1]
    part = width // lax.axis_size("tp")
    cap = (3 * toks * top_count + 2 * n_ep - 1) // (2 * n_ep)
    dma = pltpu.SemaphoreType.DMA
    return pl.pallas_call(
        fused_kernel,
        out_shape=(jax.ShapeDtypeStruct((count, part), bf16), jax.ShapeDtypeStruct((toks, part), bf16)),
        in_specs=[pl.BlockSpec(memory_space=pl.ANY)] * 14,
        out_specs=(pl.BlockSpec(memory_space=pltpu.VMEM), pl.BlockSpec(memory_space=pltpu.VMEM)),
        scratch_shapes=[
            pltpu.VMEM((count, channels), bf16),
            pltpu.VMEM((channels // dim, dim, dim), bf16),
            pltpu.VMEM((1, channels), f32),
            pltpu.VMEM(out_proj.shape, bf16),
            pltpu.VMEM((toks, width), bf16),
            pltpu.VMEM((1, width), f32),
            pltpu.VMEM((top_count, toks), jnp.int32),
            pltpu.VMEM((top_count, toks), f32),
            pltpu.VMEM(expert_gate.shape[1:], bf16),
            pltpu.VMEM(expert_up.shape[1:], bf16),
            pltpu.VMEM(expert_down.shape[1:], bf16),
            pltpu.VMEM(shared_gate.shape, bf16),
            pltpu.VMEM(shared_up.shape, bf16),
            pltpu.VMEM(shared_down.shape, bf16),
            pltpu.VMEM((HALO, channels), bf16),
            pltpu.VMEM((HALO + count, channels), f32),
            pltpu.VMEM((count, channels), bf16),
            pltpu.VMEM((count, width), bf16),
            pltpu.VMEM((2, count, part), bf16),
            pltpu.VMEM((count, part), bf16),
            pltpu.VMEM((count, part), bf16),
            pltpu.VMEM((Z_SIDE * toks, width), bf16),
            pltpu.VMEM((n_ep * cap, width), bf16),
            pltpu.VMEM((Z_SIDE * cap, width), bf16),
            pltpu.VMEM((Z_SIDE, n_ep, toks), f32),
            pltpu.VMEM((Z_SIDE, n_ep, toks), f32),
            pltpu.VMEM((Z_SIDE, X_SIDE * cap, toks), bf16),
            pltpu.VMEM((Z_SIDE, toks, X_SIDE * cap), bf16),
            pltpu.VMEM((n_ep * cap, expert_down.shape[1]), bf16),
            pltpu.VMEM((Z_SIDE, cap, part), bf16),
            pltpu.VMEM((Z_SIDE, X_SIDE * cap, part), bf16),
            pltpu.VMEM((toks, part), f32),
            pltpu.VMEM((Z_SIDE, toks, part), bf16),
            pltpu.VMEM((Z_SIDE, toks, part), bf16),
            pltpu.VMEM((toks, width), bf16),
            pltpu.VMEM((2, toks, part), bf16),
            pltpu.VMEM((toks, part), bf16),
            pltpu.VMEM((toks, part), bf16),
            dma((14,)), dma((2,)),
            dma((5, 2)), dma((4, 2)), dma((4, 2)), dma((4, 2)), dma((4, 2)), dma((4, 2)),
            dma((4, 2)), dma((4, 2)), dma((4,)), dma((4,)), dma((4, 3)), dma((4, 3)),
            dma((4, 2)), dma((4, 2)), dma((4, 2)), dma((4, 2)), dma((2, 3)), dma((2, 3)),
            dma((MIX_PARTS,)), dma((MIX_PARTS,)),
        ],
        compiler_params=pltpu.CompilerParams(
            collective_id=0, has_side_effects=True, vmem_limit_bytes=60 * 1024 * 1024),
    )(
        pool_input, pool_map, pool_scale.reshape(1, -1), out_proj, moe_input, norm_gain.reshape(1, -1),
        routes.T, route_weights.T, expert_gate, expert_up, expert_down, shared_gate, shared_up, shared_down,
    )


def solution(mesh):
    plane = mesh.shape["ep"] == Z_SIDE * X_SIDE and mesh.shape["tp"] == Y_SIDE * CORES
    body = per_device_fused if plane else per_device
    return jax.shard_map(
        body,
        mesh=mesh,
        in_specs=(
            P("ep", "tp"),
            P(),
            P(),
            P("tp", None),
            P("ep", None),
            P(),
            P("ep", None),
            P("ep", None),
            P("ep", None, "tp"),
            P("ep", None, "tp"),
            P("ep", None, "tp"),
            P(None, "tp"),
            P(None, "tp"),
            P("tp", None),
        ),
        out_specs=(P("ep", "tp"), P("ep", "tp")),
        check_vma=False,
    )
```

time: 102 us -> 80.5 us (0.79)
  Pallas kernels: 95.3 us -> 76.1 us
  other arithmetic: 1.3 us -> 0 us
    pallas_call x1, Pallas kernels: 95.3 us -> 76.1 us  [per_device_fused(): pl.pallas_call(fused_kernel, out_shape=(jax.ShapeDtypeStruct((count, part...]
    reduce_sum x1 -> x0, other arithmetic: 1.3 us -> none  [per_device_fused(): jnp.sum(jnp.where(routes[None, :, :] == ids[:, None, None], route_weights...]
where the time goes in v1:
time: 80.5 us; the launch traced here: 80.3 us
  Pallas kernels  76.1 us (95%)
  local copies, waits for them, and re-layouts  3.54 us (4%)
    pallas_call x1, Pallas kernels, per_device_fused(): pl.pallas_call(fused_kernel, out_shape=(jax.ShapeDtypeStruct((count, part...  76.1 us
    unnamed x2, local copies, waits for them, and re-layouts  3.54 us

profile of v1, /device:TPU:0, one launch (start us, length us, event | category | flops | bytes accessed | tf_op | source)
XLA Modules:
  0.0 80.3 jit_solution(3177670068044168181)
XLA Ops:
  0.6 76.1 %shard_map.149 = (bf16[256,1024]{1,0:T(8,128)(2,1)}, bf16[128,1024]{1,0:T(8,128)(2,1)}) custom-call(bf16[256,512]{1,0:T(8,128)(2,1)} %pool_h.1, bf16[16,128,128]{2,1,0:T(8,128)(2,1)} %map_h.1, f32[1,2048]{1,0:T(1,128)} %bitcast.5, bf16[512,4096]{1,0:T(8,128)(2,1)} %proj_h.1, bf16[128,4096]{1,0:T(8,128)(2,1)} %moe_h.1, f32[1,4096]{1,0:T(1,128)} %bitcast.4, ...), custom_call_target="tpu_custom_call" | custom-call | tf_op jit(solution)/shard_map/pallas_call | solution.py:661
  76.8 1.9 %copy.18 = bf16[256,1024]{1,0:T(8,128)(2,1)} copy(bf16[256,1024]{1,0:T(8,128)(2,1)} %get-tuple-element.4) | data formatting | bytes 1048576
  78.6 1.7 %copy.19 = bf16[128,1024]{1,0:T(8,128)(2,1)} copy(bf16[128,1024]{1,0:T(8,128)(2,1)} %get-tuple-element.5) | data formatting | bytes 524288

commit v2 on v1

--- a/solution.py
+++ b/solution.py
@@ -385,16 +385,19 @@
             z_wait(3, i)
             rows_out(k, i)
 
-    def early():
+    def early(i):
         @pl.when(inner)
         def _():
-            for i in (0, 1):
-                rows_out(3, i)
+            if i:
+                out_push(1)
+            rows_out(3, i)
 
     def late(i):
         @pl.when(jnp.logical_not(inner))
         def _():
             z_piece(3, i)
+            if i:
+                out_push(1)
 
     def x_piece(k, i):
         c0, n = spans()[i]
@@ -402,52 +405,68 @@
         if i == 0:
             near_push(k, 1)
 
-    def pair_ref(k, s):
-        if k == 0:
-            return comp_v.at[pl.ds(row0(0, 1), cap), pl.ds(col(s), part)]
-        return comp_v.at[pl.ds(pair_row(k), X_SIDE * cap), pl.ds(col(s), part)]
-
-    def y_arrive(k):
-        for j in (0, 1):
-            if k or j:
-                arrived(near_ref(k, j, ty), y_send.at[k, j], y_recv.at[k, j])
+    def span(u):
+        if u < 3:
+            return pair_row(u), X_SIDE * cap
+        return row0(3, u - 3), cap
+
+    def part_ref(u, s):
+        r, n = (row0(0, 1), cap) if u == 0 else span(u)
+        return comp_v.at[pl.ds(r, n), pl.ds(col(s), part)]
+
+    def y_arrive(u):
+        k = min(u, 3)
+        for j in (0, 1) if 0 < u < 3 else (1,) if u == 0 else (u - 3,):
+            arrived(near_ref(k, j, ty), y_send.at[k, j], y_recv.at[k, j])
         for i, s in enumerate((t, ty)):
-            push(pair_ref(k, s), pair_ref(k, s), c_send.at[k, i], c_recv.at[k, i], e, tc)
-
-    def core_arrive(k):
+            push(part_ref(u, s), part_ref(u, s), c_send.at[u, i], c_recv.at[u, i], e, tc)
+
+    def core_arrive(u):
         for i, s in enumerate((tc, tyc)):
-            arrived(pair_ref(k, s), c_send.at[k, i], c_recv.at[k, i])
-
-    def hid_ref(k, s):
-        return hid_v.at[pl.ds(pair_row(k), X_SIDE * cap), pl.ds(pl.multiple_of(s * hid, 128), hid)]
-
-    def expert_in(k):
-        rows = comp_v[pl.ds(pair_row(k), X_SIDE * cap), :]
+            arrived(part_ref(u, s), c_send.at[u, i], c_recv.at[u, i])
+
+    def hid_ref(u, s):
+        r, n = span(u)
+        return hid_v.at[pl.ds(r, n), pl.ds(pl.multiple_of(s * hid, 128), hid)]
+
+    def expert_in(u):
+        r, n = span(u)
+        rows = comp_v[pl.ds(r, n), :]
         g = jnp.dot(rows, gate_v[...], preferred_element_type=f32)
-        u = jnp.dot(rows, up_v[...], preferred_element_type=f32)
-        hid_ref(k, t)[...] = (g / (1.0 + jnp.exp(-g)) * u).astype(bf16)
-        push(hid_ref(k, t), hid_ref(k, t), h_send.at[k, 0], h_recv.at[k, 0], e, ty)
-        push(hid_ref(k, t), hid_ref(k, t), h_send.at[k, 1], h_recv.at[k, 1], e, tc)
-
-    def hid_forward(k):
-        arrived(hid_ref(k, ty), h_send.at[k, 0], h_recv.at[k, 0])
-        push(hid_ref(k, ty), hid_ref(k, ty), h_send.at[k, 2], h_recv.at[k, 2], e, tc)
+        u_val = jnp.dot(rows, up_v[...], preferred_element_type=f32)
+        hid_ref(u, t)[...] = (g / (1.0 + jnp.exp(-g)) * u_val).astype(bf16)
+        push(hid_ref(u, t), hid_ref(u, t), h_send.at[u, 0], h_recv.at[u, 0], e, ty)
+        push(hid_ref(u, t), hid_ref(u, t), h_send.at[u, 1], h_recv.at[u, 1], e, tc)
+
+    def hid_forward(u):
+        arrived(hid_ref(u, ty), h_send.at[u, 0], h_recv.at[u, 0])
+        push(hid_ref(u, ty), hid_ref(u, ty), h_send.at[u, 2], h_recv.at[u, 2], e, tc)
 
     half = part // 2
 
+    def half_copy(k, h):
+        cols = pl.ds(h * half, half)
+        return remote(outx_v.at[k, :, cols], pair_v.at[k, pl.ds(cap, cap), cols], rx_send.at[k, h],
+                      rx_recv.at[k, h], ex, t)
+
     def half_push(k, h):
-        cols = pl.ds(h * half, half)
-        push(outx_v.at[k, :, cols], pair_v.at[k, pl.ds(cap, cap), cols], rx_send.at[k, h],
-             rx_recv.at[k, h], ex, t)
+        go = start if k != 1 else lambda cp: cp.start()
+        go(half_copy(k, h))
+
+    def hid_wait(u):
+        arrived(hid_ref(u, tc), h_send.at[u, 1], h_recv.at[u, 1])
+        arrived(hid_ref(u, tyc), h_send.at[u, 2], h_recv.at[u, 2])
 
     def out_push(k):
         half_push(k, 0)
         half_push(k, 1)
 
     def expert_out(k, send=True):
-        arrived(hid_ref(k, tc), h_send.at[k, 1], h_recv.at[k, 1])
-        arrived(hid_ref(k, tyc), h_send.at[k, 2], h_recv.at[k, 2])
+        if k < 3:
+            hid_wait(k)
         for j in (1, 0):
+            if k == 3:
+                hid_wait(3 + j)
             rows = hid_v[pl.ds(row0(k, j), cap), :]
             for q in range(part // 256):
                 o = jnp.dot(rows, down_v[:, q * 256:(q + 1) * 256], preferred_element_type=f32).astype(bf16)
@@ -458,6 +477,16 @@
                 else:
                     pair_v[k, :cap, q * 256:(q + 1) * 256] = o
 
+    def rz_copy(k, h):
+        cols = pl.ds(h * half, half)
+        return remote(part_send.at[k, :, cols], part_z.at[turn[k], :, cols], rz_send.at[k, h],
+                      rz_recv.at[turn[k], h], zs[k] * X_SIDE + x, t)
+
+    def sum_first(here):
+        @pl.when(here)
+        def _():
+            sum_x(1)
+
     def sum_x(k):
         for h in (0, 1):
             cols = pl.ds(h * half, half)
@@ -465,8 +494,8 @@
             both = jnp.dot(mixw_v[turn[k]], pair_v[k, :, cols], preferred_element_type=f32)
             if k:
                 part_send[k, :, cols] = both.astype(bf16)
-                push(part_send.at[k, :, cols], part_z.at[turn[k], :, cols], rz_send.at[k, h],
-                     rz_recv.at[turn[k], h], zs[k] * X_SIDE + x, t)
+                go = start if k != 1 else lambda cp: cp.start()
+                go(rz_copy(k, h))
             else:
                 acc_v[:, cols] = both
 
@@ -588,7 +617,7 @@
     core_arrive(1)
     expert_in(1)
     z_piece(2, 1)
-    early()
+    early(0)
     hid_forward(0)
     x_piece(2, 0)
     loads["down"].wait()
@@ -598,28 +627,33 @@
     y_arrive(2)
     late(0)
     expert_out(1, False)
+    early(1)
     core_arrive(2)
     expert_in(2)
     late(1)
-    out_push(1)
+    y_arrive(3)
     x_piece(3, 0)
     hid_forward(2)
+    core_arrive(3)
+    sum_first(inner)
+    expert_in(3)
+    expert_out(2)
     x_piece(3, 1)
-    y_arrive(3)
-    expert_out(2)
-    core_arrive(3)
-    expert_in(3)
+    y_arrive(4)
+    hid_forward(3)
+    core_arrive(4)
+    expert_in(4)
     sh_push()
     mix_push(0)
     mix_push(1)
     mix_push(2)
     mix_push(3)
-    sum_x(1)
-    hid_forward(3)
+    sum_first(jnp.logical_not(inner))
+    hid_forward(4)
     sum_x(2)
     expert_out(3)
+    sum_x(3)
     out_push(0)
-    sum_x(3)
     sum_x(0)
     sh_final()
     mix_final()
@@ -630,6 +664,8 @@
         cp.wait_send()
     for i in (0, 1):
         x_copy(3, i).wait_send()
+        half_copy(1, i).wait_send()
+        rz_copy(1, i).wait_send()
     near_copy(3, 0).wait_send()
 
     @pl.when(inner)
@@ -660,7 +696,7 @@
     dma = pltpu.SemaphoreType.DMA
     return pl.pallas_call(
         fused_kernel,
-        out_shape=(jax.ShapeDtypeStruct((count, part), bf16), jax.ShapeDtypeStruct((toks, part), bf16)),
+        out_shape=(pltpu.VMEM((count, part), bf16), pltpu.VMEM((toks, part), bf16)),
         in_specs=[pl.BlockSpec(memory_space=pl.ANY)] * 14,
         out_specs=(pl.BlockSpec(memory_space=pltpu.VMEM), pl.BlockSpec(memory_space=pltpu.VMEM)),
         scratch_shapes=[
@@ -704,7 +740,7 @@
             pltpu.VMEM((toks, part), bf16),
             dma((14,)), dma((2,)),
             dma((5, 2)), dma((4, 2)), dma((4, 2)), dma((4, 2)), dma((4, 2)), dma((4, 2)),
-            dma((4, 2)), dma((4, 2)), dma((4,)), dma((4,)), dma((4, 3)), dma((4, 3)),
+            dma((5, 2)), dma((5, 2)), dma((4,)), dma((4,)), dma((5, 3)), dma((5, 3)),
             dma((4, 2)), dma((4, 2)), dma((4, 2)), dma((4, 2)), dma((2, 3)), dma((2, 3)),
             dma((MIX_PARTS,)), dma((MIX_PARTS,)),
         ],

time: 80.5 us -> 76.4 us (0.949)
  local copies, waits for them, and re-layouts: 3.54 us -> 1.5 us
  Pallas kernels: 76.1 us -> 74.1 us
    unnamed x2, local copies, waits for them, and re-layouts: 3.54 us -> 1.5 us
    pallas_call x1, Pallas kernels: 76.1 us -> 74.1 us  [per_device_fused(): pl.pallas_call(fused_kernel, out_shape=(pltpu.VMEM((count, part), bf16),...]
where the time goes in v2:
time: 76.4 us; the launch traced here: 76.2 us
  Pallas kernels  74.1 us (97%)
  local copies, waits for them, and re-layouts  1.5 us (2%)
    pallas_call x1, Pallas kernels, per_device_fused(): pl.pallas_call(fused_kernel, out_shape=(pltpu.VMEM((count, part), bf16),...  74.1 us

profile of v2, /device:TPU:0, one launch (start us, length us, event | category | flops | bytes accessed | tf_op | source)
XLA Modules:
  0.0 76.2 jit_solution(8230838765448115118)
XLA Ops:
  0.6 74.1 %shard_map.149 = (bf16[256,1024]{1,0:T(8,128)(2,1)S(1)}, bf16[128,1024]{1,0:T(8,128)(2,1)S(1)}) custom-call(bf16[256,512]{1,0:T(8,128)(2,1)} %pool_h.1, bf16[16,128,128]{2,1,0:T(8,128)(2,1)} %map_h.1, f32[1,2048]{1,0:T(1,128)} %bitcast.5, bf16[512,4096]{1,0:T(8,128)(2,1)} %proj_h.1, bf16[128,4096]{1,0:T(8,128)(2,1)} %moe_h.1, f32[1,4096]{1,0:T(1,128)} %bitcast.4, ...), custom_call_target="tpu_custom_call" | custom-call | tf_op jit(solution)/shard_map/pallas_call | solution.py:697
  74.7 0.8 %copy.18 = bf16[256,1024]{1,0:T(8,128)(2,1)} copy(bf16[256,1024]{1,0:T(8,128)(2,1)S(1)} %get-tuple-element.2) | data formatting | bytes 1048576
  75.5 0.7 copy.19

commit v3 on v2

--- a/solution.py
+++ b/solution.py
@@ -285,7 +285,7 @@
         halo_copy(e + 1).start()
 
     def spans():
-        return ((col(t), part), (col(ty, near), rest))
+        return ((col(t), near), (col(t, near), rest), (col(ty, near), rest))
 
     def raw_ref(k, i):
         c0, n = spans()[i]
@@ -302,7 +302,7 @@
         handed.append((k, to, at, slot, i))
         hop(k, to, at, slot, i).start()
 
-    for i in (0, 1):
+    for i in range(3):
         cp = hop(0, 1, 1, 0, i)
         cp.start()
         sent.append(cp)
@@ -339,7 +339,7 @@
         start(near_copy(k, j))
 
     routing(0)
-    for i in (0, 1):
+    for i in range(3):
         gather(0, i)
         x_push(0, i)
 
@@ -388,7 +388,7 @@
     def early(i):
         @pl.when(inner)
         def _():
-            if i:
+            if i == 2:
                 out_push(1)
             rows_out(3, i)
 
@@ -396,7 +396,7 @@
         @pl.when(jnp.logical_not(inner))
         def _():
             z_piece(3, i)
-            if i:
+            if i == 2:
                 out_push(1)
 
     def x_piece(k, i):
@@ -482,10 +482,10 @@
         return remote(part_send.at[k, :, cols], part_z.at[turn[k], :, cols], rz_send.at[k, h],
                       rz_recv.at[turn[k], h], zs[k] * X_SIDE + x, t)
 
-    def sum_first(here):
+    def sum_when(k, here):
         @pl.when(here)
         def _():
-            sum_x(1)
+            sum_x(k)
 
     def sum_x(k):
         for h in (0, 1):
@@ -494,7 +494,7 @@
             both = jnp.dot(mixw_v[turn[k]], pair_v[k, :, cols], preferred_element_type=f32)
             if k:
                 part_send[k, :, cols] = both.astype(bf16)
-                go = start if k != 1 else lambda cp: cp.start()
+                go = start if k == 3 else lambda cp: cp.start()
                 go(rz_copy(k, h))
             else:
                 acc_v[:, cols] = both
@@ -594,6 +594,7 @@
         loads["gate"].wait()
         loads["up"].wait()
 
+    outer = jnp.logical_not(inner)
     shared()
     w_arrive(1)
     w_arrive(2)
@@ -602,44 +603,52 @@
     sh_core_sum()
     proj()
     x_piece(0, 0)
-    mix_core_sum()
     z_piece(1, 0)
     x_piece(0, 1)
+    mix_core_sum()
     z_piece(1, 1)
+    x_piece(0, 2)
     y_arrive(0)
+    z_piece(1, 2)
     x_piece(1, 0)
     core_arrive(0)
     experts_loaded()
     expert_in(0)
     z_piece(2, 0)
     x_piece(1, 1)
+    x_piece(1, 2)
     y_arrive(1)
+    z_piece(2, 1)
+    x_piece(2, 0)
     core_arrive(1)
     expert_in(1)
-    z_piece(2, 1)
+    hid_forward(0)
+    z_piece(2, 2)
     early(0)
-    hid_forward(0)
-    x_piece(2, 0)
+    early(1)
+    x_piece(2, 1)
     loads["down"].wait()
     expert_out(0, False)
+    late(0)
+    x_piece(2, 2)
     hid_forward(1)
-    x_piece(2, 1)
     y_arrive(2)
-    late(0)
+    late(1)
     expert_out(1, False)
-    early(1)
+    early(2)
     core_arrive(2)
+    x_piece(3, 0)
     expert_in(2)
-    late(1)
+    late(2)
     y_arrive(3)
-    x_piece(3, 0)
+    x_piece(3, 1)
+    core_arrive(3)
     hid_forward(2)
-    core_arrive(3)
-    sum_first(inner)
+    sum_when(1, inner)
     expert_in(3)
+    x_piece(3, 2)
+    y_arrive(4)
     expert_out(2)
-    x_piece(3, 1)
-    y_arrive(4)
     hid_forward(3)
     core_arrive(4)
     expert_in(4)
@@ -648,10 +657,11 @@
     mix_push(1)
     mix_push(2)
     mix_push(3)
-    sum_first(jnp.logical_not(inner))
+    sum_when(1, outer)
+    sum_when(2, inner)
     hid_forward(4)
-    sum_x(2)
     expert_out(3)
+    sum_when(2, outer)
     sum_x(3)
     out_push(0)
     sum_x(0)
@@ -662,10 +672,12 @@
 
     for cp in sent:
         cp.wait_send()
+    for i in range(3):
+        x_copy(3, i).wait_send()
     for i in (0, 1):
-        x_copy(3, i).wait_send()
         half_copy(1, i).wait_send()
         rz_copy(1, i).wait_send()
+        rz_copy(2, i).wait_send()
     near_copy(3, 0).wait_send()
 
     @pl.when(inner)
@@ -678,7 +690,7 @@
         halo_copy(e + 1).wait_send()
 
 
-NEAR = 2
+NEAR = 4
 
 
 def per_device_fused(
@@ -739,7 +751,7 @@
             pltpu.VMEM((toks, part), bf16),
             pltpu.VMEM((toks, part), bf16),
             dma((14,)), dma((2,)),
-            dma((5, 2)), dma((4, 2)), dma((4, 2)), dma((4, 2)), dma((4, 2)), dma((4, 2)),
+            dma((5, 3)), dma((5, 3)), dma((4, 3)), dma((4, 3)), dma((4, 2)), dma((4, 2)),
             dma((5, 2)), dma((5, 2)), dma((4,)), dma((4,)), dma((5, 3)), dma((5, 3)),
             dma((4, 2)), dma((4, 2)), dma((4, 2)), dma((4, 2)), dma((2, 3)), dma((2, 3)),
             dma((MIX_PARTS,)), dma((MIX_PARTS,)),

time: 76.4 us -> 71 us (0.929)
  Pallas kernels: 74.1 us -> 68.7 us
    pallas_call x1, Pallas kernels: 74.1 us -> 68.7 us  [per_device_fused(): pl.pallas_call(fused_kernel, out_shape=(pltpu.VMEM((count, part), bf16),...]
where the time goes in v3:
time: 71 us; the launch traced here: 70.9 us
  Pallas kernels  68.7 us (97%)
  local copies, waits for them, and re-layouts  1.5 us (2%)
    pallas_call x1, Pallas kernels, per_device_fused(): pl.pallas_call(fused_kernel, out_shape=(pltpu.VMEM((count, part), bf16),...  68.7 us
    unnamed x2, local copies, waits for them, and re-layouts  1.5 us

profile of v3, /device:TPU:0, one launch (start us, length us, event | category | flops | bytes accessed | tf_op | source)
XLA Modules:
  0.0 70.9 jit_solution(17866532846346574819)
XLA Ops:
  0.6 68.7 %shard_map.149 = (bf16[256,1024]{1,0:T(8,128)(2,1)S(1)}, bf16[128,1024]{1,0:T(8,128)(2,1)S(1)}) custom-call(bf16[256,512]{1,0:T(8,128)(2,1)} %pool_h.1, bf16[16,128,128]{2,1,0:T(8,128)(2,1)} %map_h.1, f32[1,2048]{1,0:T(1,128)} %bitcast.5, bf16[512,4096]{1,0:T(8,128)(2,1)} %proj_h.1, bf16[128,4096]{1,0:T(8,128)(2,1)} %moe_h.1, f32[1,4096]{1,0:T(1,128)} %bitcast.4, ...), custom_call_target="tpu_custom_call" | custom-call | tf_op jit(solution)/shard_map/pallas_call | solution.py:709
  69.4 0.8 %copy.18 = bf16[256,1024]{1,0:T(8,128)(2,1)} copy(bf16[256,1024]{1,0:T(8,128)(2,1)S(1)} %get-tuple-element.2) | data formatting | bytes 1048576
  70.2 0.7 copy.19

commit v4 on v3

--- a/solution.py
+++ b/solution.py
@@ -256,7 +256,7 @@
         raw_v[pl.ds(own + r, 16), :] = (cen * lax.rsqrt(var + eps) * gain_v[...]).astype(bf16)
         return carry
 
-    lax.fori_loop(0, toks // 16, norm_step, 0, unroll=2)
+    lax.fori_loop(0, toks // 16, norm_step, 0, unroll=4)
     loads["pool"].wait()
     loads["route"].wait()
     loads["rw"].wait()
@@ -364,8 +364,6 @@
         go = start if k < 3 else lambda cp: cp.start()
         gather(k, i)
         go(x_copy(k, i))
-        if i == 0:
-            go(near_copy(k, 0))
 
     def z_piece(k, i):
         if k < 3:
@@ -604,6 +602,7 @@
     proj()
     x_piece(0, 0)
     z_piece(1, 0)
+    near_push(1, 0)
     x_piece(0, 1)
     mix_core_sum()
     z_piece(1, 1)
@@ -615,6 +614,7 @@
     experts_loaded()
     expert_in(0)
     z_piece(2, 0)
+    near_push(2, 0)
     x_piece(1, 1)
     x_piece(1, 2)
     y_arrive(1)
@@ -632,6 +632,7 @@
     late(0)
     x_piece(2, 2)
     hid_forward(1)
+    near_push(3, 0)
     y_arrive(2)
     late(1)
     expert_out(1, False)
@@ -646,9 +647,9 @@
     hid_forward(2)
     sum_when(1, inner)
     expert_in(3)
+    expert_out(2)
     x_piece(3, 2)
     y_arrive(4)
-    expert_out(2)
     hid_forward(3)
     core_arrive(4)
     expert_in(4)
@@ -678,7 +679,6 @@
         half_copy(1, i).wait_send()
         rz_copy(1, i).wait_send()
         rz_copy(2, i).wait_send()
-    near_copy(3, 0).wait_send()
 
     @pl.when(inner)
     def _():

time: 71 us -> 69.9 us (0.985)
  Pallas kernels: 68.7 us -> 67.6 us
    pallas_call x1, Pallas kernels: 68.7 us -> 67.6 us  [per_device_fused(): pl.pallas_call(fused_kernel, out_shape=(pltpu.VMEM((count, part), bf16),...]
where the time goes in v4:
time: 69.9 us; the launch traced here: 69.7 us
  Pallas kernels  67.6 us (97%)
  local copies, waits for them, and re-layouts  1.5 us (2%)
    pallas_call x1, Pallas kernels, per_device_fused(): pl.pallas_call(fused_kernel, out_shape=(pltpu.VMEM((count, part), bf16),...  67.6 us
    unnamed x2, local copies, waits for them, and re-layouts  1.5 us

profile of v4, /device:TPU:0, one launch (start us, length us, event | category | flops | bytes accessed | tf_op | source)
XLA Modules:
  0.0 69.7 jit_solution(1111845206813140505)
XLA Ops:
  0.6 67.6 %shard_map.149 = (bf16[256,1024]{1,0:T(8,128)(2,1)S(1)}, bf16[128,1024]{1,0:T(8,128)(2,1)S(1)}) custom-call(bf16[256,512]{1,0:T(8,128)(2,1)} %pool_h.1, bf16[16,128,128]{2,1,0:T(8,128)(2,1)} %map_h.1, f32[1,2048]{1,0:T(1,128)} %bitcast.5, bf16[512,4096]{1,0:T(8,128)(2,1)} %proj_h.1, bf16[128,4096]{1,0:T(8,128)(2,1)} %moe_h.1, f32[1,4096]{1,0:T(1,128)} %bitcast.4, ...), custom_call_target="tpu_custom_call" | custom-call | tf_op jit(solution)/shard_map/pallas_call | solution.py:709
  68.2 0.8 %copy.18 = bf16[256,1024]{1,0:T(8,128)(2,1)} copy(bf16[256,1024]{1,0:T(8,128)(2,1)S(1)} %get-tuple-element.2) | data formatting | bytes 1048576
  69.0 0.7 %copy.19 = bf16[128,1024]{1,0:T(8,128)(2,1)} copy(bf16[128,1024]{1,0:T(8,128)(2,1)S(1)} %get-tuple-element.3) | data formatting | bytes 524288

commit v5 on v4

--- a/solution.py
+++ b/solution.py
@@ -644,6 +644,7 @@
     y_arrive(3)
     x_piece(3, 1)
     core_arrive(3)
+    mix_push(0)
     hid_forward(2)
     sum_when(1, inner)
     expert_in(3)
@@ -654,7 +655,6 @@
     core_arrive(4)
     expert_in(4)
     sh_push()
-    mix_push(0)
     mix_push(1)
     mix_push(2)
     mix_push(3)

time: 69.9 us -> 70 us (level)
  no operation moved by 1% of the time
where the time goes in v5:
time: 70 us; the launch traced here: 69.9 us
  Pallas kernels  67.7 us (97%)
  local copies, waits for them, and re-layouts  1.5 us (2%)
    pallas_call x1, Pallas kernels, per_device_fused(): pl.pallas_call(fused_kernel, out_shape=(pltpu.VMEM((count, part), bf16),...  67.7 us
    unnamed x2, local copies, waits for them, and re-layouts  1.5 us

profile of v5, /device:TPU:0, one launch (start us, length us, event | category | flops | bytes accessed | tf_op | source)
XLA Modules:
  0.0 69.9 jit_solution(10492999440689847437)
XLA Ops:
  0.6 67.7 %shard_map.149 = (bf16[256,1024]{1,0:T(8,128)(2,1)S(1)}, bf16[128,1024]{1,0:T(8,128)(2,1)S(1)}) custom-call(bf16[256,512]{1,0:T(8,128)(2,1)} %pool_h.1, bf16[16,128,128]{2,1,0:T(8,128)(2,1)} %map_h.1, f32[1,2048]{1,0:T(1,128)} %bitcast.5, bf16[512,4096]{1,0:T(8,128)(2,1)} %proj_h.1, bf16[128,4096]{1,0:T(8,128)(2,1)} %moe_h.1, f32[1,4096]{1,0:T(1,128)} %bitcast.4, ...), custom_call_target="tpu_custom_call" | custom-call | tf_op jit(solution)/shard_map/pallas_call | solution.py:709
  68.4 0.8 %copy.18 = bf16[256,1024]{1,0:T(8,128)(2,1)} copy(bf16[256,1024]{1,0:T(8,128)(2,1)S(1)} %get-tuple-element.2) | data formatting | bytes 1048576
  69.1 0.7 %copy.19 = bf16[128,1024]{1,0:T(8,128)(2,1)} copy(bf16[128,1024]{1,0:T(8,128)(2,1)S(1)} %get-tuple-element.3) | data formatting | bytes 524288
